TPU v7x, 32 devices: a whole 2x2x4 slice. The times are simulated.
32 devices in a mesh: fs: 4 (over z), rep: 4 (over y, x), tp: 2 (over core).
Axes of the slice: x: 2, y: 2, z: 4, core: 2. Of those that a mesh axis runs over, the one named last changes fastest.
Arguments:
- saved_inputs: bfloat16 [12288, 2048], P(('fs', 'rep')), may hold values from -6 to 6
- query_cotangent: bfloat16 [12288, 1024], P(('fs', 'rep'), 'tp'), may hold values from -0.053955078 to 0.053955078
- value_cotangent: bfloat16 [12288, 2048], P(('fs', 'rep'), 'tp'), may hold values from -0.053955078 to 0.053955078
- query_weight: float32 [2048, 1024], P('fs', 'tp'), may hold values from -0.125 to 0.125
- value_weight: float32 [2048, 2048], P('fs', 'tp'), may hold values from -0.125 to 0.125
- query_factor: bfloat16 [2048, 256], P('fs'), as said below
- value_factor: bfloat16 [2048, 256], P('fs'), as said below
- query_first: float32 [256, 1024], P('rep', 'tp'), may hold values from -6 to 6
- query_second: float32 [256, 1024], P('rep', 'tp'), may hold values from 0.3 to 3
- value_first: float32 [256, 2048], P('rep', 'tp'), may hold values from -6 to 6
- value_second: float32 [256, 2048], P('rep', 'tp'), may hold values from 0.3 to 3
Outputs:
- query_direction: float32 [2048, 1024], P('fs', 'tp')
- value_direction: float32 [2048, 2048], P('fs', 'tp')
- query_master: float32 [2048, 1024], P('fs', 'tp')
- value_master: float32 [2048, 2048], P('fs', 'tp')
- query_first_new: float32 [256, 1024], P('rep', 'tp')
- query_second_new: float32 [256, 1024], P('rep', 'tp')
- value_first_new: float32 [256, 2048], P('rep', 'tp')
- value_second_new: float32 [256, 2048], P('rep', 'tp')
- query_copy: bfloat16 [2048, 1024], P(None, 'tp')
- value_copy: bfloat16 [2048, 2048], P(None, 'tp')
Inputs may be any that keep to these rules, and one draw needn't show every extreme that they name: `query_factor`: A matrix of full rank. `value_factor`: A matrix of full rank.
All inputs are finite; a program needn't handle non-finite values.
Results may differ from a plain program's by a relative error of at most 0.012.
Values may be sent and summed in bfloat16 or wider, within the bound.
A program may use at most 128 MiB of HBM per device.

v0:
```python
import jax
import jax.numpy as jnp
from jax import lax
from jax.sharding import PartitionSpec as P

BETA_ONE = 0.8
BETA_TWO = 0.9
EPS_RATIO = 1e-08
EPS_NORM = 1e-06
RATE = 0.02


def moments(projected, first, second):
    first_new = BETA_ONE * first + (1.0 - BETA_ONE) * projected
    second_new = BETA_TWO * second + (1.0 - BETA_TWO) * projected * projected
    ratio = first_new / (jnp.sqrt(second_new) + EPS_RATIO)
    return (first_new, second_new, ratio)


def local(
    saved_inputs,
    query_cotangent,
    value_cotangent,
    query_weight,
    value_weight,
    query_factor,
    value_factor,
    query_first,
    query_second,
    value_first,
    value_second,
):
    qc = query_cotangent.shape[1]
    rank = query_factor.shape[1]
    rows = query_weight.shape[0]
    tp = lax.axis_size("tp")
    bf = jnp.bfloat16
    f32 = jnp.float32
    dims = (((0,), (0,)), ((), ()))
    factors = lax.all_gather(
        jnp.concatenate([query_factor, value_factor], axis=1), "fs", axis=0, tiled=True
    )
    weights = lax.all_gather(
        jnp.concatenate([query_weight.astype(bf), value_weight.astype(bf)], axis=1),
        "fs",
        axis=0,
        tiled=True,
    )
    low = jnp.dot(saved_inputs, factors, preferred_element_type=f32).astype(bf)
    proj = jnp.concatenate(
        [
            lax.dot_general(low[:, :rank], query_cotangent, dims, preferred_element_type=f32),
            lax.dot_general(low[:, rank:], value_cotangent, dims, preferred_element_type=f32),
        ],
        axis=1,
    )
    proj = lax.psum_scatter(proj.astype(bf), "rep", scatter_dimension=0, tiled=True)
    proj = lax.psum(proj.astype(f32), "fs")
    query_first_new, query_second_new, query_ratio = moments(
        proj[:, :qc], query_first, query_second
    )
    value_first_new, value_second_new, value_ratio = moments(
        proj[:, qc:], value_first, value_second
    )
    ratio = jnp.concatenate([query_ratio.astype(bf), value_ratio.astype(bf)], axis=1)
    ratio = lax.all_gather(ratio, "rep", axis=0, tiled=True)
    query_raw = jnp.dot(factors[:, :rank], ratio[:, :qc], preferred_element_type=f32)
    value_raw = jnp.dot(factors[:, rank:], ratio[:, qc:], preferred_element_type=f32)
    query_total, value_total = lax.psum(
        (jnp.sum(query_raw * query_raw), jnp.sum(value_raw * value_raw)), "tp"
    )
    query_scale = lax.rsqrt(query_total / (query_raw.size * tp) + EPS_NORM)
    value_scale = lax.rsqrt(value_total / (value_raw.size * tp) + EPS_NORM)
    query_copy = (weights[:, :qc].astype(f32) - RATE * (query_raw * query_scale)).astype(bf)
    value_copy = (weights[:, qc:].astype(f32) - RATE * (value_raw * value_scale)).astype(bf)
    start = lax.axis_index("fs") * rows
    query_direction = lax.dynamic_slice_in_dim(query_raw, start, rows, 0) * query_scale
    value_direction = lax.dynamic_slice_in_dim(value_raw, start, rows, 0) * value_scale
    query_master = query_weight - RATE * query_direction
    value_master = value_weight - RATE * value_direction
    return (
        query_direction,
        value_direction,
        query_master,
        value_master,
        query_first_new,
        query_second_new,
        value_first_new,
        value_second_new,
        query_copy,
        value_copy,
    )


def solution(mesh):
    return jax.shard_map(
        local,
        mesh=mesh,
        in_specs=(
            P(("fs", "rep"), None),
            P(("fs", "rep"), "tp"),
            P(("fs", "rep"), "tp"),
            P("fs", "tp"),
            P("fs", "tp"),
            P("fs", None),
            P("fs", None),
            P("rep", "tp"),
            P("rep", "tp"),
            P("rep", "tp"),
            P("rep", "tp"),
        ),
        out_specs=(
            P("fs", "tp"),
            P("fs", "tp"),
            P("fs", "tp"),
            P("fs", "tp"),
            P("rep", "tp"),
            P("rep", "tp"),
            P("rep", "tp"),
            P("rep", "tp"),
            P(None, "tp"),
            P(None, "tp"),
        ),
        check_vma=False,
    )
```

profile of v0, /device:TPU:0, one launch (start us, length us, event | category | flops | bytes accessed | tf_op | source)
XLA Modules:
  0.0 285.0 jit_solution(16459601803138328107)
XLA Ops:
  7.2 0.0 copy-start
  7.2 0.0 all-gather.3.cloned.1.call-start
  7.2 2.0 pad_maximum_fusion.2
  9.2 0.0 all-gather.3.cloned.1.call-update
  9.3 0.0 reduce-scatter.2.cloned.1.call-start
  9.3 49.2 %all-gather.3.cloned.1.call-done = bf16[2048,512]{1,0:T(8,128)(2,1)} async-done(((bf16[512,512]{1,0:T(8,128)(2,1)}), bf16[2048,512]{1,0:T(8,128)(2,1)}) %all-gather.3.cloned.1.call-update) | async-done | bytes 2097168 | tf_op jit(solution)/shard_map/all_gather | solution.py:40
  58.6 0.0 copy-done
  58.6 0.0 copy-start.4
  58.6 0.0 copy-start.5
  58.6 3.6 %fusion = bf16[768,512]{0,1:T(8,128)(2,1)S(1)} fusion(bf16[2048,512]{1,0:T(8,128)(2,1)} %all-gather.3.cloned.1.call-done, bf16[768,2048]{1,0:T(8,128)(2,1)S(1)} %copy-done), kind=kOutput, calls=%fused_computation.8 | convolution fusion | flops 1611005952 | bytes 6029312 | tf_op jit(solution)/shard_map/dot_general | solution.py:49
  62.1 0.0 copy-done.4
  62.2 0.6 convolution_convert_fusion.1
  62.7 0.0 copy-done.5
  62.8 0.4 convolution_convert_fusion.2
  63.1 0.9 pad_maximum_fusion.1
  64.1 0.0 reduce-scatter.2.cloned.1.call-update
  64.1 0.0 all-gather.5.cloned.1.call-start
  64.1 25.1 %reduce-scatter.2.cloned.1.call-done = bf16[64,1536]{1,0:T(8,128)(2,1)} async-done(((bf16[256,1536]{1,0:T(8,128)(2,1)}), bf16[64,1536]{1,0:T(8,128)(2,1)}) %reduce-scatter.2.cloned.1.call-update) | async-done | bytes 196624 | tf_op jit(solution)/shard_map/reduce_scatter | solution.py:57
  89.2 26.9 %all-reduce.2 = f32[64,1536]{1,0:T(8,128)S(1)} all-reduce(bf16[64,1536]{1,0:T(8,128)(2,1)} %reduce-scatter.2.cloned.1.call-done), channel_id=1, replica_groups=mesh['fs'=4,'rep'=4,'tp'=2] {'fs'}, use_global_device_ids=true, to_apply=%region_1.0 | all-reduce | flops 98304 | bytes 589824 | tf_op jit(solution)/shard_map/psum | solution.py:58
  116.1 0.0 copy-start.2
  116.1 2.1 divide_convert_fusion
  118.2 1.7 divide_convert_fusion.1
  120.0 11.0 %all_gather.10 = bf16[256,1536]{1,0:T(8,128)(2,1)S(1)} all-gather(bf16[64,1536]{1,0:T(8,128)(2,1)S(1)} %pad_maximum_fusion.3), channel_id=1, replica_groups=mesh['fs'=4,'rep'=4,'tp'=2] {'rep'}, dimensions={0}, use_global_device_ids=true | all-gather | bytes 983040 | tf_op jit(solution)/shard_map/all_gather | solution.py:66
  131.0 0.0 copy-done.2
  131.0 3.8 %multiply_reduce_fusion.1 = (f32[]{:T(128)}, f32[2048,512]{1,0:T(8,128)}) fusion(bf16[256,1536]{1,0:T(8,128)(2,1)S(1)} %all_gather.10, bf16[2048,512]{1,0:T(8,128)(2,1)S(1)} %copy-done.2), kind=kOutput, calls=%fused_computation.3 | convolution fusion | flops 538968064 | bytes 5505028 | tf_op jit(solution)/shard_map/dot_general | solution.py:67
  134.8 6.1 %multiply_reduce_fusion = (f32[]{:T(128)}, f32[2048,1024]{1,0:T(8,128)}) fusion(bf16[256,1536]{1,0:T(8,128)(2,1)S(1)} %all_gather.10, bf16[2048,512]{1,0:T(8,128)(2,1)S(1)} %copy-done.2), kind=kOutput, calls=%fused_computation.1 | convolution fusion | flops 1077936128 | bytes 9961476 | tf_op jit(solution)/shard_map/dot_general | solution.py:68
  140.9 3.1 %all-reduce = (f32[]{:T(128)}, f32[]{:T(128)}) all-reduce(f32[]{:T(128)} %get-tuple-element.24, f32[]{:T(128)} %get-tuple-element.26), channel_id=1, replica_groups=mesh['fs'=4,'rep'=4,'tp'=2] {'tp'}, use_global_device_ids=true, to_apply=%region_3.0 | all-reduce | flops 2 | bytes 16 | tf_op jit(solution)/shard_map/psum | solution.py:69
  145.4 0.0 copy-start.3
  145.4 3.6 %multiply_subtract_fusion.1 = (f32[512,512]{1,0:T(8,128)}, f32[512,512]{1,0:T(8,128)}, bf16[512,512]{1,0:T(8,128)(2,1)S(1)}) fusion(f32[512,512]{1,0:T(8,128)} %param.14, f32[]{:T(128)S(6)} %rsqrt.6, f32[2048,512]{1,0:T(8,128)} %get-tuple-element.25, s32[]{:T(128)S(6)} %select_n.4), kind=kLoop, calls=%fused_computation.15 | loop fusion | flops 1048576 | bytes 4718600 | tf_op jit(solution)/shard_map/sub | solution.py:79
  149.0 0.0 copy-done.3
  149.0 4.6 %multiply_subtract_fusion = (f32[512,1024]{1,0:T(8,128)}, f32[512,1024]{1,0:T(8,128)}, bf16[512,1024]{1,0:T(8,128)(2,1)S(1)}) fusion(f32[512,1024]{1,0:T(8,128)S(1)} %copy-done.3, f32[]{:T(128)S(6)} %rsqrt.7, f32[2048,1024]{1,0:T(8,128)} %get-tuple-element.27, s32[]{:T(128)S(6)} %select_n.4), kind=kLoop, calls=%fused_computation.4 | loop fusion | flops 2097152 | bytes 9437192 | tf_op jit(solution)/shard_map/sub | solution.py:80
  153.6 1.2 pad_maximum_fusion
  154.8 0.0 all-gather.5.cloned.1.call-update
  154.9 112.9 %all-gather.5.cloned.1.call-done = bf16[2048,1536]{1,0:T(8,128)(2,1)} async-done(((bf16[512,1536]{1,0:T(8,128)(2,1)}), bf16[2048,1536]{1,0:T(8,128)(2,1)}) %all-gather.5.cloned.1.call-update) | async-done | bytes 6291472 | tf_op jit(solution)/shard_map/all_gather | solution.py:43
  267.7 0.0 copy-start.1
  267.7 5.1 %subtract_convert_fusion.1 = bf16[2048,512]{1,0:T(8,128)(2,1)} fusion(f32[2048,512]{1,0:T(8,128)} %get-tuple-element.25, bf16[2048,1536]{1,0:T(8,128)(2,1)} %all-gather.5.cloned.1.call-done, f32[]{:T(128)S(6)} %rsqrt.6), kind=kLoop, calls=%fused_computation.2 | loop fusion | flops 5242880 | bytes 8388612 | tf_op jit(solution)/shard_map/convert_element_type | solution.py:74
  272.8 0.0 copy-done.1
  272.8 5.7 %subtract_convert_fusion = bf16[2048,1024]{1,0:T(8,128)(2,1)} fusion(f32[2048,1024]{1,0:T(8,128)} %get-tuple-element.27, bf16[2048,1536]{1,0:T(8,128)(2,1)S(1)} %copy-done.1, f32[]{:T(128)S(6)} %rsqrt.7), kind=kLoop, calls=%fused_computation | loop fusion | flops 10485760 | bytes 16777220 | tf_op jit(solution)/shard_map/convert_element_type | solution.py:75
  (1 shorter events, 0.0 us)
Async XLA Ops:
  7.2 51.4 %copy-start = (bf16[768,2048]{1,0:T(8,128)(2,1)S(1)}, bf16[768,2048]{1,0:T(8,128)(2,1)}, u32[]{:S(2)}) copy-start(bf16[768,2048]{1,0:T(8,128)(2,1)} %param.11) | copy-start | bytes 9437188
  7.2 51.4 %all-gather.3.cloned.1.call-start = ((), (), s32[]{:S(2)}) async-start(), calls=%async_computation.1 | async-start | bytes 2621440 | tf_op jit(solution)/shard_map/all_gather | solution.py:40
  9.3 79.9 %reduce-scatter.2.cloned.1.call-start = ((), (), s32[]{:S(2)}) async-start(), calls=%async_computation.2 | async-start | bytes 983040 | tf_op jit(solution)/shard_map/reduce_scatter | solution.py:57
  58.6 3.6 %copy-start.4 = (bf16[768,1024]{1,0:T(8,128)(2,1)S(1)}, bf16[768,1024]{1,0:T(8,128)(2,1)}, u32[]{:S(2)}) copy-start(bf16[768,1024]{1,0:T(8,128)(2,1)} %param.13) | copy-start | bytes 4718596
  58.6 4.2 %copy-start.5 = (bf16[768,512]{1,0:T(8,128)(2,1)S(1)}, bf16[768,512]{1,0:T(8,128)(2,1)}, u32[]{:S(2)}) copy-start(bf16[768,512]{1,0:T(8,128)(2,1)} %param.12) | copy-start | bytes 2359300
  64.1 203.7 %all-gather.5.cloned.1.call-start = ((), (), s32[]{:S(2)}) async-start(), calls=%async_computation.3 | async-start | bytes 7864320 | tf_op jit(solution)/shard_map/all_gather | solution.py:43
  116.1 14.9 %copy-start.2 = (bf16[2048,512]{1,0:T(8,128)(2,1)S(1)}, bf16[2048,512]{1,0:T(8,128)(2,1)}, u32[]{:S(2)}) copy-start(bf16[2048,512]{1,0:T(8,128)(2,1)} %all-gather.3.cloned.1.call-done) | copy-start | bytes 6291460
  145.4 3.7 %copy-start.3 = (f32[512,1024]{1,0:T(8,128)S(1)}, f32[512,1024]{1,0:T(8,128)}, u32[]{:S(2)}) copy-start(f32[512,1024]{1,0:T(8,128)} %param.15) | copy-start | bytes 6291460
  267.7 5.1 %copy-start.1 = (bf16[2048,1536]{1,0:T(8,128)(2,1)S(1)}, bf16[2048,1536]{1,0:T(8,128)(2,1)}, u32[]{:S(2)}) copy-start(bf16[2048,1536]{1,0:T(8,128)(2,1)} %all-gather.5.cloned.1.call-done) | copy-start | bytes 18874372
Sparse Core Ops, SparseCore 0:
  10.1 48.3 all-gather.2
  64.2 24.9 reduce-scatter.1
  155.0 112.7 all-gather.4
where the time goes:
time: 285 us
  waiting for transfers between devices  187 us (66%)
  blocking collectives  41.1 us (14%)
  other arithmetic  27 us (9%)
  between operations  15.2 us (5%)
  matrix products  14.4 us (5%)
    all_gather x1, waiting for transfers between devices, local(): lax.all_gather(jnp.concatenate([query_weight.astype(bf), value_weight.ast...  113 us
    all_gather x1, waiting for transfers between devices, local(): lax.all_gather(jnp.concatenate([query_factor, value_factor], axis=1), 'fs...  49.2 us
    psum x1, blocking collectives, local(): proj = lax.psum(proj.astype(f32), 'fs')  26.9 us
    reduce_scatter x1, waiting for transfers between devices, local(): lax.psum_scatter(proj.astype(bf), 'rep', scatter_dimension=0, tiled=True)  25.1 us
    all_gather x1, blocking collectives, local(): ratio = lax.all_gather(ratio, 'rep', axis=0, tiled=True)  11 us
    dot_general x1, matrix products, local(): jnp.dot(factors[:, rank:], ratio[:, qc:], preferred_element_type=f32)  6.09 us
  transfers between devices with their start and end apart: 3, of which 3 were waited for; matrix products, arithmetic and copies ran while one was open for 0% of the time, Pallas kernels for 0%

commit v1 on v0

--- a/solution.py
+++ b/solution.py
@@ -55,7 +55,7 @@
         axis=1,
     )
     proj = lax.psum_scatter(proj.astype(bf), "rep", scatter_dimension=0, tiled=True)
-    proj = lax.psum(proj.astype(f32), "fs")
+    proj = jnp.sum(lax.all_gather(proj.astype(f32), "fs"), axis=0)
     query_first_new, query_second_new, query_ratio = moments(
         proj[:, :qc], query_first, query_second
     )

time: 285 us -> 300 us (1.053)
  waiting for transfers between devices: 187 us -> 226 us
  blocking collectives: 41.1 us -> 14.1 us
  other arithmetic: 27 us -> 30.2 us
    all_gather x0 -> x1, waiting for transfers between devices: none -> 37.4 us  [local(): proj = jnp.sum(lax.all_gather(proj.astype(f32), 'fs'), axis=0)]
    psum x1 -> x0, blocking collectives: 26.9 us -> none  [local(): proj = lax.psum(proj.astype(f32), 'fs')]
  transfers between devices with their start and end apart: 3 -> 4, of which waited for: 3 -> 4; matrix products, arithmetic and copies ran while one was open for 0% -> 0% of each run, Pallas kernels for 0% -> 0%
where the time goes in v1:
time: 300 us
  waiting for transfers between devices  226 us (75%)
  other arithmetic  30.2 us (10%)
  between operations  15.2 us (5%)
  matrix products  14.4 us (5%)
  blocking collectives  14.1 us (5%)
    all_gather x1, waiting for transfers between devices, local(): lax.all_gather(jnp.concatenate([query_weight.astype(bf), value_weight.ast...  114 us
    all_gather x1, waiting for transfers between devices, local(): lax.all_gather(jnp.concatenate([query_factor, value_factor], axis=1), 'fs...  49.2 us
    all_gather x1, waiting for transfers between devices, local(): proj = jnp.sum(lax.all_gather(proj.astype(f32), 'fs'), axis=0)  37.4 us
    reduce_scatter x1, waiting for transfers between devices, local(): lax.psum_scatter(proj.astype(bf), 'rep', scatter_dimension=0, tiled=True)  25.1 us
    all_gather x1, blocking collectives, local(): ratio = lax.all_gather(ratio, 'rep', axis=0, tiled=True)  11.1 us
    dot_general x1, matrix products, local(): jnp.dot(factors[:, rank:], ratio[:, qc:], preferred_element_type=f32)  6.07 us
  transfers between devices with their start and end apart: 4, of which 4 were waited for; matrix products, arithmetic and copies ran while one was open for 0% of the time, Pallas kernels for 0%

profile of v1, /device:TPU:0, one launch (start us, length us, event | category | flops | bytes accessed | tf_op | source)
XLA Modules:
  0.0 299.9 jit_solution(15829503786949996288)
XLA Ops:
  7.2 0.0 copy-start
  7.2 0.0 all-gather.5.cloned.1.call-start
  7.2 2.0 pad_maximum_fusion.2
  9.2 0.0 all-gather.5.cloned.1.call-update
  9.3 0.0 reduce-scatter.2.cloned.1.call-start
  9.3 49.2 %all-gather.5.cloned.1.call-done = bf16[2048,512]{1,0:T(8,128)(2,1)} async-done(((bf16[512,512]{1,0:T(8,128)(2,1)}), bf16[2048,512]{1,0:T(8,128)(2,1)}) %all-gather.5.cloned.1.call-update) | async-done | bytes 2097168 | tf_op jit(solution)/shard_map/all_gather | solution.py:40
  58.6 0.0 copy-done
  58.6 0.0 copy-start.4
  58.6 0.0 copy-start.5
  58.6 3.6 %fusion = bf16[768,512]{0,1:T(8,128)(2,1)S(1)} fusion(bf16[2048,512]{1,0:T(8,128)(2,1)} %all-gather.5.cloned.1.call-done, bf16[768,2048]{1,0:T(8,128)(2,1)S(1)} %copy-done), kind=kOutput, calls=%fused_computation.8 | convolution fusion | flops 1611005952 | bytes 6029312 | tf_op jit(solution)/shard_map/dot_general | solution.py:49
  62.1 0.0 copy-done.4
  62.2 0.6 convolution_convert_fusion.1
  62.7 0.0 copy-done.5
  62.8 0.4 convolution_convert_fusion.2
  63.1 0.9 pad_maximum_fusion.1
  64.1 0.0 reduce-scatter.2.cloned.1.call-update
  64.1 0.0 all-gather.9.cloned.1.call-start
  64.1 25.1 %reduce-scatter.2.cloned.1.call-done = bf16[64,1536]{1,0:T(8,128)(2,1)} async-done(((bf16[256,1536]{1,0:T(8,128)(2,1)}), bf16[64,1536]{1,0:T(8,128)(2,1)}) %reduce-scatter.2.cloned.1.call-update) | async-done | bytes 196624 | tf_op jit(solution)/shard_map/reduce_scatter | solution.py:57
  89.2 1.7 all_gather.24
  90.9 0.0 all-gather.9.cloned.1.call-update
  90.9 0.0 all-gather.7.cloned.1.call-start
  91.0 37.4 %all-gather.9.cloned.1.call-done = f32[256,1536]{1,0:T(8,128)} async-done(((f32[64,1536]{1,0:T(8,128)}), f32[256,1536]{1,0:T(8,128)}) %all-gather.9.cloned.1.call-update) | async-done | bytes 1572880 | tf_op jit(solution)/shard_map/all_gather | solution.py:58
  128.4 1.5 reduce_sum.27
  129.9 0.0 copy-start.2
  129.9 2.1 divide_convert_fusion
  132.0 1.7 divide_convert_fusion.1
  133.8 11.1 %all_gather.22 = bf16[256,1536]{1,0:T(8,128)(2,1)S(1)} all-gather(bf16[64,1536]{1,0:T(8,128)(2,1)S(1)} %pad_maximum_fusion.3), channel_id=1, replica_groups=mesh['fs'=4,'rep'=4,'tp'=2] {'rep'}, dimensions={0}, use_global_device_ids=true | all-gather | bytes 983040 | tf_op jit(solution)/shard_map/all_gather | solution.py:66
  144.8 0.0 copy-done.2
  144.8 3.8 %multiply_reduce_fusion.1 = (f32[]{:T(128)}, f32[2048,512]{1,0:T(8,128)}) fusion(bf16[256,1536]{1,0:T(8,128)(2,1)S(1)} %all_gather.22, bf16[2048,512]{1,0:T(8,128)(2,1)S(1)} %copy-done.2), kind=kOutput, calls=%fused_computation.3 | convolution fusion | flops 538968064 | bytes 5505028 | tf_op jit(solution)/shard_map/dot_general | solution.py:67
  148.6 6.1 %multiply_reduce_fusion = (f32[]{:T(128)}, f32[2048,1024]{1,0:T(8,128)}) fusion(bf16[256,1536]{1,0:T(8,128)(2,1)S(1)} %all_gather.22, bf16[2048,512]{1,0:T(8,128)(2,1)S(1)} %copy-done.2), kind=kOutput, calls=%fused_computation.1 | convolution fusion | flops 1077936128 | bytes 9961476 | tf_op jit(solution)/shard_map/dot_general | solution.py:68
  154.7 3.1 %all-reduce = (f32[]{:T(128)}, f32[]{:T(128)}) all-reduce(f32[]{:T(128)} %get-tuple-element.24, f32[]{:T(128)} %get-tuple-element.26), channel_id=1, replica_groups=mesh['fs'=4,'rep'=4,'tp'=2] {'tp'}, use_global_device_ids=true, to_apply=%region_3.0 | all-reduce | flops 2 | bytes 16 | tf_op jit(solution)/shard_map/psum | solution.py:69
  159.2 0.0 copy-start.3
  159.2 3.6 %multiply_subtract_fusion.1 = (f32[512,512]{1,0:T(8,128)}, f32[512,512]{1,0:T(8,128)}, bf16[512,512]{1,0:T(8,128)(2,1)S(1)}) fusion(f32[512,512]{1,0:T(8,128)} %param.14, f32[]{:T(128)S(6)} %rsqrt.6, f32[2048,512]{1,0:T(8,128)} %get-tuple-element.25, s32[]{:T(128)S(6)} %select_n.4), kind=kLoop, calls=%fused_computation.15 | loop fusion | flops 1048576 | bytes 4718600 | tf_op jit(solution)/shard_map/sub | solution.py:79
  162.8 0.0 copy-done.3
  162.8 4.6 %multiply_subtract_fusion = (f32[512,1024]{1,0:T(8,128)}, f32[512,1024]{1,0:T(8,128)}, bf16[512,1024]{1,0:T(8,128)(2,1)S(1)}) fusion(f32[512,1024]{1,0:T(8,128)S(1)} %copy-done.3, f32[]{:T(128)S(6)} %rsqrt.7, f32[2048,1024]{1,0:T(8,128)} %get-tuple-element.27, s32[]{:T(128)S(6)} %select_n.4), kind=kLoop, calls=%fused_computation.4 | loop fusion | flops 2097152 | bytes 9437192 | tf_op jit(solution)/shard_map/sub | solution.py:80
  167.4 1.2 pad_maximum_fusion
  168.6 0.0 all-gather.7.cloned.1.call-update
  168.7 113.9 %all-gather.7.cloned.1.call-done = bf16[2048,1536]{1,0:T(8,128)(2,1)} async-done(((bf16[512,1536]{1,0:T(8,128)(2,1)}), bf16[2048,1536]{1,0:T(8,128)(2,1)}) %all-gather.7.cloned.1.call-update) | async-done | bytes 6291472 | tf_op jit(solution)/shard_map/all_gather | solution.py:43
  282.6 0.0 copy-start.1
  282.6 5.1 %subtract_convert_fusion.1 = bf16[2048,512]{1,0:T(8,128)(2,1)} fusion(f32[2048,512]{1,0:T(8,128)} %get-tuple-element.25, bf16[2048,1536]{1,0:T(8,128)(2,1)} %all-gather.7.cloned.1.call-done, f32[]{:T(128)S(6)} %rsqrt.6), kind=kLoop, calls=%fused_computation.2 | loop fusion | flops 5242880 | bytes 8388612 | tf_op jit(solution)/shard_map/convert_element_type | solution.py:74
  287.7 0.0 copy-done.1
  287.7 5.7 %subtract_convert_fusion = bf16[2048,1024]{1,0:T(8,128)(2,1)} fusion(f32[2048,1024]{1,0:T(8,128)} %get-tuple-element.27, bf16[2048,1536]{1,0:T(8,128)(2,1)S(1)} %copy-done.1, f32[]{:T(128)S(6)} %rsqrt.7), kind=kLoop, calls=%fused_computation | loop fusion | flops 10485760 | bytes 16777220 | tf_op jit(solution)/shard_map/convert_element_type | solution.py:75
  (1 shorter events, 0.0 us)
Async XLA Ops:
  7.2 51.4 %copy-start = (bf16[768,2048]{1,0:T(8,128)(2,1)S(1)}, bf16[768,2048]{1,0:T(8,128)(2,1)}, u32[]{:S(2)}) copy-start(bf16[768,2048]{1,0:T(8,128)(2,1)} %param.11) | copy-start | bytes 9437188
  7.2 51.4 %all-gather.5.cloned.1.call-start = ((), (), s32[]{:S(2)}) async-start(), calls=%async_computation.1 | async-start | bytes 2621440 | tf_op jit(solution)/shard_map/all_gather | solution.py:40
  9.3 79.9 %reduce-scatter.2.cloned.1.call-start = ((), (), s32[]{:S(2)}) async-start(), calls=%async_computation.2 | async-start | bytes 983040 | tf_op jit(solution)/shard_map/reduce_scatter | solution.py:57
  58.6 3.6 %copy-start.4 = (bf16[768,1024]{1,0:T(8,128)(2,1)S(1)}, bf16[768,1024]{1,0:T(8,128)(2,1)}, u32[]{:S(2)}) copy-start(bf16[768,1024]{1,0:T(8,128)(2,1)} %param.13) | copy-start | bytes 4718596
  58.6 4.2 %copy-start.5 = (bf16[768,512]{1,0:T(8,128)(2,1)S(1)}, bf16[768,512]{1,0:T(8,128)(2,1)}, u32[]{:S(2)}) copy-start(bf16[768,512]{1,0:T(8,128)(2,1)} %param.12) | copy-start | bytes 2359300
  64.1 64.3 %all-gather.9.cloned.1.call-start = ((), (), s32[]{:S(2)}) async-start(), calls=%async_computation.4 | async-start | bytes 1966080 | tf_op jit(solution)/shard_map/all_gather | solution.py:58
  90.9 191.7 %all-gather.7.cloned.1.call-start = ((), (), s32[]{:S(2)}) async-start(), calls=%async_computation.3 | async-start | bytes 7864320 | tf_op jit(solution)/shard_map/all_gather | solution.py:43
  129.9 14.9 %copy-start.2 = (bf16[2048,512]{1,0:T(8,128)(2,1)S(1)}, bf16[2048,512]{1,0:T(8,128)(2,1)}, u32[]{:S(2)}) copy-start(bf16[2048,512]{1,0:T(8,128)(2,1)} %all-gather.5.cloned.1.call-done) | copy-start | bytes 6291460
  159.2 3.7 %copy-start.3 = (f32[512,1024]{1,0:T(8,128)S(1)}, f32[512,1024]{1,0:T(8,128)}, u32[]{:S(2)}) copy-start(f32[512,1024]{1,0:T(8,128)} %param.15) | copy-start | bytes 6291460
  282.6 5.1 %copy-start.1 = (bf16[2048,1536]{1,0:T(8,128)(2,1)S(1)}, bf16[2048,1536]{1,0:T(8,128)(2,1)}, u32[]{:S(2)}) copy-start(bf16[2048,1536]{1,0:T(8,128)(2,1)} %all-gather.7.cloned.1.call-done) | copy-start | bytes 18874372
Sparse Core Ops, SparseCore 0:
  10.1 48.3 all-gather.4
  64.2 24.9 reduce-scatter.1
  91.3 36.9 all-gather.8
  168.8 113.7 all-gather.6
